TPU v7x, 32 devices: a whole 2x2x4 slice. The times are simulated.
32 devices in a mesh: gr: 2 (over x), fs: 8 (over z, y), tp: 2 (over core).
Axes of the slice: x: 2, y: 2, z: 4, core: 2. Of those that a mesh axis runs over, the one named last changes fastest.
Arguments:
- tokens: bfloat16 [4096, 2048], P(('gr', 'tp'), 'fs'), may hold values from -400 to 400
- norm_gain: float32 [2048], P('fs'), may hold values from 0.1 to 1.9
- up_weight: float32 [2048, 8192], P('fs', ('gr', 'tp')), may hold values from -0.125 to 0.125
- down_weight: float32 [8192, 2048], P('fs', ('gr', 'tp')), may hold values from -0.09375 to 0.09375
Outputs:
- mixed: bfloat16 [2048, 4096], P('fs', ('gr', 'tp'))
- up_ready: bfloat16 [2048, 8192], P(None, 'fs')
- down_ready: bfloat16 [8192, 2048], P('fs')
All inputs are finite; a program needn't handle non-finite values.
Results may differ from a plain program's by a relative error of at most 0.023.
Values may be sent and summed in bfloat16 or wider, within the bound.
A program may use at most 64 MiB of HBM per device.

v0:
```python
import jax
import jax.numpy as jnp
from jax import lax
from jax.sharding import PartitionSpec as P

epsilon = 1e-06


def shards(tokens, norm_gain, up_weight, down_weight):
    folded = (norm_gain[:, None] * up_weight).astype(jnp.bfloat16)
    down_cast = down_weight.astype(jnp.bfloat16)
    fs_count = lax.axis_size("fs")
    group_count = lax.axis_size(("gr", "tp"))
    rows_here, cols_here = folded.shape
    sub_rows = rows_here // group_count
    row_groups = folded.reshape(group_count, sub_rows, cols_here)
    full_rows = lax.all_to_all(row_groups, ("gr", "tp"), split_axis=0, concat_axis=2, tiled=True)
    full_width = full_rows.shape[2]
    unit_width = full_width // fs_count
    by_unit = full_rows.reshape(1, sub_rows, fs_count, unit_width)
    by_owner = lax.all_to_all(by_unit, "fs", split_axis=2, concat_axis=0, tiled=True)
    arranged = by_owner.reshape(fs_count, 1, sub_rows, unit_width)
    stacked, down_full = (
        lax.all_gather(arranged, ("gr", "tp"), axis=1, tiled=True),
        lax.all_gather(down_cast, ("gr", "tp"), axis=1, tiled=True),
    )
    up_full = stacked.reshape(fs_count * group_count * sub_rows, unit_width)
    model_width = up_full.shape[0]
    piece = lax.all_gather(tokens, "fs", axis=1, tiled=True)
    running = jnp.dot(piece, up_full, preferred_element_type=jnp.float32)
    piece_wide = piece.astype(jnp.float32)
    squares = jnp.sum(piece_wide * piece_wide, axis=1)
    raw_up, squares = (running, squares)
    row_scale = lax.rsqrt(squares / model_width + epsilon)
    hidden = jnp.square(jax.nn.relu(raw_up * row_scale[:, None])).astype(jnp.bfloat16)
    outcome = lax.psum_scatter(
        lax.dot_general(
            down_full, hidden, (((0,), (1,)), ((), ())), preferred_element_type=jnp.float32
        ).astype(jnp.bfloat16),
        "fs",
        scatter_dimension=0,
        tiled=True,
    )
    return (outcome, up_full, down_full)


def solution(mesh):
    in_specs = (P(("gr", "tp"), "fs"), P("fs"), P("fs", ("gr", "tp")), P("fs", ("gr", "tp")))
    out_specs = (P("fs", ("gr", "tp")), P(None, "fs"), P("fs", None))
    return jax.shard_map(shards, mesh=mesh, in_specs=in_specs, out_specs=out_specs, check_vma=False)
```

profile of v0, /device:TPU:0, one launch (start us, length us, event | category | flops | bytes accessed | tf_op | source)
XLA Modules:
  0.0 292.2 jit_solution(18041260175511250311)
XLA Ops:
  7.2 0.0 all-gather.5.cloned.1.call-start
  7.2 0.7 all-gather.5.cloned.1.call-update
  7.9 0.0 all-gather.9.cloned.1.call-start
  7.9 1.8 multiply_convert_fusion.1
  9.7 18.5 %all_to_all.30 = bf16[4,64,2048]{2,1,0:T(8,128)(2,1)S(1)} all-to-all(bf16[4,64,2048]{2,1,0:T(8,128)(2,1)S(1)} %bitcast.19), channel_id=1, replica_groups=mesh['gr'=2,'fs'=8,'tp'=2] {'gr','tp'}, dimensions={0} | all-to-all | bytes 2097152 | tf_op jit(solution)/shard_map/all_to_all | solution.py:17
  28.2 0.8 copy.13
  29.0 0.3 reshape.27
  29.3 0.6 copy.14
  29.9 0.0 copy-start
  29.9 53.7 %all_to_all.31 = bf16[1,64,8,1024]{3,1,0,2:T(8,128)(2,1)} all-to-all(bf16[1,64,8,1024]{3,1,0,2:T(8,128)(2,1)S(1)} %copy.14), channel_id=1, replica_groups=mesh['gr'=2,'fs'=8,'tp'=2] {'fs'}, dimensions={2} | all-to-all | bytes 2097152 | tf_op jit(solution)/shard_map/all_to_all | solution.py:21
  83.6 0.0 all-gather.9.cloned.1.call-update
  83.6 0.0 all-gather.7.cloned.1.call-start
  83.7 0.0 copy-done
  83.7 1.1 convert_element_type.22
  84.8 0.0 all-gather.7.cloned.1.call-update
  84.8 0.0 reduce-scatter.2.cloned.1.call-start
  84.9 18.0 %all-gather.5.cloned.1.call-done = bf16[1024,2048]{1,0:T(8,128)(2,1)} async-done(((bf16[1024,256]{1,0:T(8,128)(2,1)}), bf16[1024,2048]{1,0:T(8,128)(2,1)}) %all-gather.5.cloned.1.call-update) | async-done | bytes 4194320 | tf_op jit(solution)/shard_map/all_gather | solution.py:29
  102.8 3.1 %multiply_reduce_fusion = f32[1024]{0:T(1024)S(1)} fusion(bf16[1024,2048]{1,0:T(8,128)(2,1)} %all-gather.5.cloned.1.call-done), kind=kLoop, calls=%fused_computation | loop fusion | flops 6290432 | bytes 4198400 | tf_op jit(solution)/shard_map/reduce_sum | solution.py:32
  105.9 32.9 %all-gather.9.cloned.1.call-done = bf16[8,4,64,1,1024]{4,2,3,0,1:T(8,128)(2,1)} async-done(((bf16[8,1,64,1,1024]{4,2,3,0,1:T(8,128)(2,1)}), bf16[8,4,64,1,1024]{4,2,3,0,1:T(8,128)(2,1)}) %all-gather.9.cloned.1.call-update) | async-done | bytes 4194320 | tf_op jit(solution)/shard_map/all_gather | solution.py:24
  138.8 4.9 %copy.16 = bf16[8,4,64,1,1024]{4,2,1,0,3:T(8,128)(2,1)} copy(bf16[8,4,64,1,1024]{4,2,3,0,1:T(8,128)(2,1)} %all-gather.9.cloned.1.call-done) | data formatting | bytes 8388608 | tf_op jit(solution)/shard_map/all_gather | solution.py:24
  143.7 31.7 %all-gather.7.cloned.1.call-done = bf16[1024,2048]{1,0:T(8,128)(2,1)} async-done(((bf16[1024,512]{1,0:T(8,128)(2,1)}), bf16[1024,2048]{1,0:T(8,128)(2,1)}) %all-gather.7.cloned.1.call-update) | async-done | bytes 4194320 | tf_op jit(solution)/shard_map/all_gather | solution.py:25
  175.5 14.5 %convert_bitcast_fusion = bf16[2048,1024]{0,1:T(8,128)(2,1)} fusion(bf16[1024,2048]{1,0:T(8,128)(2,1)} %all-gather.7.cloned.1.call-done, bf16[2048,1024]{1,0:T(8,128)(2,1)} %bitcast.15, bf16[1024,2048]{1,0:T(8,128)(2,1)} %all-gather.5.cloned.1.call-done, f32[1024]{0:T(1024)S(1)} %add_rsqrt_fusion), kind=kOutput, calls=%fused_computation.1 | convolution fusion | flops 8596226048 | bytes 16781312 | tf_op jit(solution)/shard_map/dot_general | solution.py:37
  190.0 0.0 reduce-scatter.2.cloned.1.call-update
  190.0 88.8 %reduce-scatter.2.cloned.1.call-done = bf16[256,1024]{0,1:T(8,128)(2,1)} async-done(((bf16[2048,1024]{0,1:T(8,128)(2,1)}), bf16[256,1024]{0,1:T(8,128)(2,1)}) %reduce-scatter.2.cloned.1.call-update) | async-done | bytes 524304 | tf_op jit(solution)/shard_map/reduce_scatter | solution.py:36
  278.8 2.0 copy.17
  280.9 4.8 %copy.19 = bf16[1024,2048]{1,0:T(8,128)(2,1)} copy(bf16[1024,2048]{1,0:T(8,128)(2,1)} %all-gather.7.cloned.1.call-done) | data formatting | bytes 8388608
  (1 shorter events, 0.0 us)
Async XLA Ops:
  7.2 95.7 %all-gather.5.cloned.1.call-start = ((), (), s32[]{:S(2)}) async-start(), calls=%async_computation.3 | async-start | bytes 4718592 | tf_op jit(solution)/shard_map/all_gather | solution.py:29
  7.9 130.9 %all-gather.9.cloned.1.call-start = ((), (), s32[]{:S(2)}) async-start(), calls=%async_computation.6 | async-start | bytes 5242880 | tf_op jit(solution)/shard_map/all_gather | solution.py:24
  29.9 53.8 %copy-start = (f32[1024,512]{1,0:T(8,128)S(1)}, f32[1024,512]{1,0:T(8,128)}, u32[]{:S(2)}) copy-start(f32[1024,512]{1,0:T(8,128)} %param.7) | copy-start | bytes 6291460
  83.6 91.8 %all-gather.7.cloned.1.call-start = ((), (), s32[]{:S(2)}) async-start(), calls=%async_computation.4 | async-start | bytes 5242880 | tf_op jit(solution)/shard_map/all_gather | solution.py:25
  84.8 194.0 %reduce-scatter.2.cloned.1.call-start = ((), (), s32[]{:S(2)}) async-start(), calls=%async_computation.5 | async-start | bytes 4718592 | tf_op jit(solution)/shard_map/reduce_scatter | solution.py:36
Sparse Core Ops, SparseCore 0:
  10.0 92.7 all-gather.4
  104.4 34.3 all-gather.8
  141.0 34.4 all-gather.6
  190.1 88.6 reduce-scatter.1
where the time goes:
time: 293 us; the launch traced here: 292 us
  waiting for transfers between devices  172 us (59%)
  blocking collectives  72.2 us (25%)
  matrix products  14.5 us (5%)
  between operations  13.8 us (5%)
  local copies, waits for them, and re-layouts  13.4 us (5%)
  other arithmetic  5.95 us (2%)
    reduce_scatter x1, waiting for transfers between devices, shards(): lax.psum_scatter(lax.dot_general(down_full, hidden, (((0,), (1,)), ((), (...  88.8 us
    all_to_all x1, blocking collectives, shards(): lax.all_to_all(by_unit, 'fs', split_axis=2, concat_axis=0, tiled=True)  53.7 us
    all_gather x1, waiting for transfers between devices, shards(): lax.all_gather(arranged, ('gr', 'tp'), axis=1, tiled=True)  32.9 us
    all_gather x1, waiting for transfers between devices, shards(): lax.all_gather(down_cast, ('gr', 'tp'), axis=1, tiled=True)  31.7 us
    all_to_all x1, blocking collectives, shards(): lax.all_to_all(row_groups, ('gr', 'tp'), split_axis=0, concat_axis=2, til...  18.5 us
    all_gather x1, waiting for transfers between devices, shards(): piece = lax.all_gather(tokens, 'fs', axis=1, tiled=True)  18 us
    dot_general x1, matrix products, shards(): lax.dot_general(down_full, hidden, (((0,), (1,)), ((), ())), preferred_el...  14.5 us
    unnamed x4, local copies, waits for them, and re-layouts  6.83 us
  transfers between devices with their start and end apart: 4, of which 4 were waited for; matrix products, arithmetic and copies ran while one was open for 4% of the time, Pallas kernels for 0%

commit v1 on v0

v1 whole, which is shorter than its diff:
```python
import functools

import jax
import jax.numpy as jnp
from jax import lax
from jax.experimental import pallas as pl
from jax.experimental.pallas import tpu as pltpu
from jax.sharding import PartitionSpec as P

MESH = pl.DeviceIdType.MESH
epsilon = 1e-06


def line_shape(count):
    short = max(d for d in range(1, count + 1) if count % d == 0 and d * d <= count)
    return count // short, short


def chunks(total, size):
    return min(total, size)


def kernel(
    G, n, T, Z, Y, k,
    tok_ref, gain_ref, upw_ref, dnw_ref,
    mixed_ref, up_out, dn_out,
    up_bf, tok_full, up_full, dn_full, hidden, part, ybuf, zup, zdn,
    tok_recv, tok_su, tok_sd, tok_sy,
    up_recv, up_s, up_sx, up_st,
    dn_recv, dn_sx, dn_st,
    y_recv, y_send, zu_recv, zu_send, zd_recv, zd_send, out_sem,
):
    g, f, t = lax.axis_index("gr"), lax.axis_index("fs"), lax.axis_index("tp")
    z, y = f // Y, f % Y
    q = g * T + t
    rows = upw_ref.shape[0]
    sub = rows // G
    unit = up_full.shape[1]
    dcols = dnw_ref.shape[1]
    pending = []

    def send(src, dst, ssem, rsem, dev, cond=None):
        copy = pltpu.make_async_remote_copy(
            src_ref=src, dst_ref=dst, send_sem=ssem, recv_sem=rsem, device_id=dev, device_id_type=MESH
        )
        if cond is None:
            copy.start()
        else:
            pl.when(cond)(copy.start)
        pending.append((cond, copy))

    def arrived(ref, sem):
        pltpu.make_async_copy(ref, ref, sem).wait()

    own = pltpu.make_async_copy(tok_ref, tok_full.at[f], tok_recv.at[f])
    own.start()

    def pass_tokens(zc, src, up, down):
        c = zc * Y + y
        dst = tok_full.at[c]
        if up is not None:
            send(src, dst, tok_su.at[zc], tok_recv.at[c], (g, f + Y, t), up)
        if down is not None:
            send(src, dst, tok_sd.at[zc], tok_recv.at[c], (g, f - Y, t), down)

    def cross_tokens(zc, src, cond):
        c = zc * Y + y
        for o in range(1, Y):
            y2 = (y + o) % Y
            send(src, tok_full.at[c], tok_sy.at[zc, o], tok_recv.at[c], (g, z * Y + y2, t), cond)

    pass_tokens(z, tok_ref, z < Z - 1, z > 0)
    cross_tokens(z, tok_ref, None)

    step = chunks(rows, 32)
    for j in range(k):
        @pl.loop(0, rows // step)
        def _(i):
            r = pl.ds(pl.multiple_of(i * step, step), step)
            up_bf[j, r, :] = (gain_ref[r, :] * upw_ref[r, pl.ds(j * unit, unit)]).astype(jnp.bfloat16)

    def piece(c, h):
        return up_full.at[pl.ds(pl.multiple_of(c * rows + h * sub, sub), sub)]

    for oh in reversed(range(G)):
        h = (g + oh) % G
        for j in range(k):
            owner = q * k + j
            src = up_bf.at[j, pl.ds(pl.multiple_of(h * sub, sub), sub)]
            if oh == 0:
                local = pltpu.make_async_copy(src, piece(f, h), up_recv.at[f, h])
                pl.when(owner == f)(local.start)
                send(src, piece(f, h), up_s.at[j, oh], up_recv.at[f, h], (h, owner, t), owner != f)
            else:
                send(src, piece(f, h), up_s.at[j, oh], up_recv.at[f, h], (h, owner, t))

    def dn_block(index):
        return dn_full.at[:, pl.ds(pl.multiple_of(index * dcols, dcols), dcols)]

    deep = dnw_ref.shape[0]
    dstep = chunks(deep, 64)

    @pl.loop(0, deep // dstep)
    def _(i):
        r = pl.ds(pl.multiple_of(i * dstep, dstep), dstep)
        dn_full[r, pl.ds(pl.multiple_of(q * dcols, dcols), dcols)] = dnw_ref[r, :].astype(jnp.bfloat16)

    for o in range(1, G):
        send(dn_block(q), dn_block(q), dn_sx.at[o], dn_recv.at[q], ((g + o) % G, f, t))
    for o in range(1, T):
        send(dn_block(q), dn_block(q), dn_st.at[0, o], dn_recv.at[q], (g, f, (t + o) % T))

    star = (f // k) % T
    is_star = t == star

    def relay_direct(c):
        @pl.when(is_star)
        def _():
            arrived(piece(c, g), up_recv.at[c, g])
        for o in range(1, G):
            send(piece(c, g), piece(c, g), up_sx.at[c, o], up_recv.at[c, g], ((g + o) % G, f, t), is_star)
        for o in range(1, T):
            send(piece(c, g), piece(c, g), up_st.at[c, 0, o], up_recv.at[c, g], (g, f, (t + o) % T), is_star)

    def relay_far(c):
        for oh in range(1, G):
            h = (g + oh) % G
            @pl.when(is_star)
            def _():
                arrived(piece(c, h), up_recv.at[c, h])
            for o in range(1, T):
                send(piece(c, h), piece(c, h), up_st.at[c, oh, o], up_recv.at[c, h], (g, f, (t + o) % T), is_star)

    earlier = []
    for s in range(Z):
        if s > 0:
            lower, upper = z - s >= 0, z + s < Z
            zl, zu = jnp.maximum(z - s, 0), jnp.minimum(z + s, Z - 1)

            @pl.when(lower)
            def _():
                arrived(tok_full.at[zl * Y + y], tok_recv.at[zl * Y + y])
            pass_tokens(zl, tok_full.at[zl * Y + y], lower & (z < Z - 1), None)
            cross_tokens(zl, tok_full.at[zl * Y + y], lower)

            @pl.when(upper)
            def _():
                arrived(tok_full.at[zu * Y + y], tok_recv.at[zu * Y + y])
            pass_tokens(zu, tok_full.at[zu * Y + y], None, upper & (z > 0))
            cross_tokens(zu, tok_full.at[zu * Y + y], upper)
        else:
            own.wait()
        zc = (z + s) % Z
        now = [zc * Y + (y + o) % Y for o in range(Y)]
        for c in now:
            relay_direct(c)
        for c in earlier:
            relay_far(c)
        earlier = now
        if s == 1 % Z:
            for o in range(1, G):
                index = ((g + o) % G) * T + t
                arrived(dn_block(index), dn_recv.at[index])
                for ot in range(1, T):
                    send(dn_block(index), dn_block(index), dn_st.at[o, ot], dn_recv.at[index], (g, f, (t + ot) % T))
    for c in earlier:
        relay_far(c)

    for zc in range(Z):
        for o in range(1, Y):
            c = zc * Y + (y + o) % Y
            arrived(tok_full.at[c], tok_recv.at[c])

    @pl.when(jnp.logical_not(is_star))
    def _():
        @pl.loop(0, n)
        def _(c):
            for h in range(G):
                arrived(piece(c, h), up_recv.at[c, h])

    up_store = pltpu.make_async_copy(up_full, up_out, out_sem.at[0])
    up_store.start()

    tokens_here = tok_ref.shape[0]
    tile = chunks(tokens_here, 256)
    width = n * tok_ref.shape[1]

    @pl.loop(0, tokens_here // tile)
    def _(i):
        r = pl.ds(pl.multiple_of(i * tile, tile), tile)
        blocks = [tok_full[c, r, :] for c in range(n)]
        squares = None
        for block in blocks:
            wide = block.astype(jnp.float32)
            total = jnp.sum(wide * wide, axis=1, keepdims=True)
            squares = total if squares is None else squares + total
        scale = lax.rsqrt(squares / width + epsilon)
        raw = jnp.dot(jnp.concatenate(blocks, axis=1), up_full[...], preferred_element_type=jnp.float32)
        hidden[r, :] = jnp.square(jnp.maximum(raw * scale, 0.0)).astype(jnp.bfloat16)

    for o in range(G):
        for ot in range(1, T):
            index = ((g + o) % G) * T + (t + ot) % T
            arrived(dn_block(index), dn_recv.at[index])
    dn_store = pltpu.make_async_copy(dn_full, dn_out, out_sem.at[1])
    dn_store.start()

    feat = part.shape[1]

    def nth(o):
        value = jnp.int32(0)
        for zv in range(Z):
            order = sorted(range(Z), key=lambda zd: (-abs(zd - zv), zd))
            value = jnp.where(z == zv, order[o], value)
        return value

    def multiply(c):
        across = dn_full[:, pl.ds(pl.multiple_of(c * feat, feat), feat)] if feat % 128 == 0 else None
        return across

    if feat % 128 == 0:
        def compute(c):
            cols = dn_full[:, pl.ds(pl.multiple_of(c * feat, feat), feat)]
            part[c] = lax.dot_general(
                cols.T, hidden[...], (((1,), (1,)), ((), ())), preferred_element_type=jnp.float32
            ).astype(jnp.bfloat16)
    else:
        per = 128 // feat

        @pl.loop(0, n // per)
        def _(b):
            cols = dn_full[:, pl.ds(pl.multiple_of(b * 128, 128), 128)]
            whole = lax.dot_general(
                cols.T, hidden[...], (((1,), (1,)), ((), ())), preferred_element_type=jnp.float32
            ).astype(jnp.bfloat16)
            for p in range(per):
                part[b * per + p] = whole[p * feat:(p + 1) * feat]

        def compute(c):
            pass

    @pl.loop(0, Z)
    def _(i):
        zd = nth_dynamic(i, z, Z)
        for o in range(1, Y):
            y2 = (y + o) % Y
            c = zd * Y + y2
            compute(c)
            pltpu.make_async_remote_copy(
                src_ref=part.at[c], dst_ref=ybuf.at[zd, Y - o], send_sem=y_send.at[zd, o],
                recv_sem=y_recv.at[zd, Y - o], device_id=(g, z * Y + y2, t), device_id_type=MESH,
            ).start()
        compute(zd * Y + y)

    for zd in range(Z):
        for o in range(1, Y):
            c = zd * Y + (y + o) % Y
            pending.append((None, pltpu.make_async_remote_copy(
                src_ref=part.at[c], dst_ref=ybuf.at[zd, Y - o], send_sem=y_send.at[zd, o],
                recv_sem=y_recv.at[zd, Y - o], device_id=(g, z * Y + (y + o) % Y, t), device_id_type=MESH,
            )))

    rstep = chunks(feat, 32)

    def add_up(zd, extras, target, start=None):
        c = zd * Y + y

        @pl.loop(0, feat // rstep)
        def _(i):
            r = pl.ds(pl.multiple_of(i * rstep, rstep), rstep)
            total = part[c, r, :].astype(jnp.float32)
            for o in range(1, Y):
                total = total + ybuf[zd, o, r, :].astype(jnp.float32)
            for extra in extras:
                total = total + extra[zd, r, :].astype(jnp.float32)
            if target is None:
                part[c, r, :] = total.astype(jnp.bfloat16)
            else:
                target[r, :] = total.astype(jnp.bfloat16)

    for i in range(Z):
        zd = nth(i)
        for o in range(1, Y):
            arrived(ybuf.at[zd, o], y_recv.at[zd, o])
        c = zd * Y + y
        going_up, going_down = zd > z, zd < z

        @pl.when(going_up & (z > 0))
        def _():
            arrived(zup.at[zd], zu_recv.at[zd])
            add_up(zd, [zup], None)

        @pl.when(going_up & (z == 0))
        def _():
            add_up(zd, [], None)

        @pl.when(going_down & (z < Z - 1))
        def _():
            arrived(zdn.at[zd], zd_recv.at[zd])
            add_up(zd, [zdn], None)

        @pl.when(going_down & (z == Z - 1))
        def _():
            add_up(zd, [], None)

        send(part.at[c], zup.at[zd], zu_send.at[zd], zu_recv.at[zd], (g, f + Y, t), going_up)
        send(part.at[c], zdn.at[zd], zd_send.at[zd], zd_recv.at[zd], (g, f - Y, t), going_down)

        @pl.when(zd == z)
        def _():
            @pl.when(z > 0)
            def _():
                arrived(zup.at[zd], zu_recv.at[zd])

            @pl.when(z < Z - 1)
            def _():
                arrived(zdn.at[zd], zd_recv.at[zd])

            @pl.when(z == 0)
            def _():
                add_up(zd, [zdn] if Z > 1 else [], mixed_ref)

            if Z > 1:
                @pl.when(z == Z - 1)
                def _():
                    add_up(zd, [zup], mixed_ref)

                @pl.when((z > 0) & (z < Z - 1))
                def _():
                    add_up(zd, [zup, zdn], mixed_ref)

    for cond, copy in pending:
        if cond is None:
            copy.wait_send()
        else:
            pl.when(cond)(copy.wait_send)
    up_store.wait()
    dn_store.wait()


def nth_dynamic(i, z, Z):
    value = jnp.int32(0)
    for zv in range(Z):
        order = sorted(range(Z), key=lambda zd: (-abs(zd - zv), zd))
        for o in range(Z):
            value = jnp.where((z == zv) & (i == o), order[o], value)
    return value


def shards(dims, tokens, norm_gain, up_weight, down_weight):
    G, n, T = dims
    Z, Y = line_shape(n)
    rows, cols = up_weight.shape
    here, w = tokens.shape
    deep, dcols = down_weight.shape
    unit = cols * G * T // n
    k = n // (G * T)
    width = rows * n
    feat = dcols * G * T // n
    bf = jnp.bfloat16
    dma = pltpu.SemaphoreType.DMA
    vmem = pl.BlockSpec(memory_space=pltpu.VMEM)
    hbm = pl.BlockSpec(memory_space=pl.ANY)
    return pl.pallas_call(
        functools.partial(kernel, G, n, T, Z, Y, k),
        out_shape=(
            jax.ShapeDtypeStruct((feat, here), bf),
            jax.ShapeDtypeStruct((width, unit), bf),
            jax.ShapeDtypeStruct((deep, dcols * G * T), bf),
        ),
        in_specs=[vmem] * 4,
        out_specs=(vmem, hbm, hbm),
        scratch_shapes=[
            pltpu.VMEM((k, rows, unit), bf),
            pltpu.VMEM((n, here, w), bf),
            pltpu.VMEM((width, unit), bf),
            pltpu.VMEM((deep, dcols * G * T), bf),
            pltpu.VMEM((here, unit), bf),
            pltpu.VMEM((n, feat, here), bf),
            pltpu.VMEM((Z, Y, feat, here), bf),
            pltpu.VMEM((Z, feat, here), bf),
            pltpu.VMEM((Z, feat, here), bf),
            dma((n,)), dma((Z,)), dma((Z,)), dma((Z, Y)),
            dma((n, G)), dma((k, G)), dma((n, G)), dma((n, G, T)),
            dma((G * T,)), dma((G,)), dma((G, T)),
            dma((Z, Y)), dma((Z, Y)), dma((Z,)), dma((Z,)), dma((Z,)), dma((Z,)), dma((2,)),
        ],
        compiler_params=pltpu.CompilerParams(has_side_effects=True, vmem_limit_bytes=60 * 1024 * 1024),
    )(tokens, norm_gain[:, None], up_weight, down_weight)


def solution(mesh):
    dims = (mesh.shape["gr"], mesh.shape["fs"], mesh.shape["tp"])
    in_specs = (P(("gr", "tp"), "fs"), P("fs"), P("fs", ("gr", "tp")), P("fs", ("gr", "tp")))
    out_specs = (P("fs", ("gr", "tp")), P(None, "fs"), P("fs", None))
    return jax.shard_map(
        functools.partial(shards, dims), mesh=mesh, in_specs=in_specs, out_specs=out_specs, check_vma=False
    )
```

time: 293 us -> 170 us (0.58)
  waiting for transfers between devices: 172 us -> 0 us
  Pallas kernels: 0 us -> 159 us
  blocking collectives: 72.2 us -> 0 us
  matrix products: 14.5 us -> 0 us
  between operations: 13.8 us -> 0.64 us
  other arithmetic: 5.95 us -> 0 us
  local copies, waits for them, and re-layouts: 13.4 us -> 10.2 us
    pallas_call x0 -> x1, Pallas kernels: none -> 159 us  [shards(): pl.pallas_call(functools.partial(kernel, G, n, T, Z, Y, k), out_shape=(ja...]
    reduce_scatter x1 -> x0, waiting for transfers between devices: 88.8 us -> none  [shards(): lax.psum_scatter(lax.dot_general(down_full, hidden, (((0,), (1,)), ((), (...]
    all_gather x3 -> x0, waiting for transfers between devices: 82.6 us -> none  [the longest x1 32.9 us: shards(): lax.all_gather(arranged, ('gr', 'tp'), axis=1, tiled=True)]
    all_to_all x2 -> x0, blocking collectives: 72.2 us -> none  [the longest x1 53.7 us: shards(): lax.all_to_all(by_unit, 'fs', split_axis=2, concat_axis=0, tiled=True)]
    dot_general x1 -> x0, matrix products: 14.5 us -> none  [shards(): lax.dot_general(down_full, hidden, (((0,), (1,)), ((), ())), preferred_el...]
    all_gather x1 -> x0, local copies, waits for them, and re-layouts: 4.91 us -> none  [shards(): lax.all_gather(arranged, ('gr', 'tp'), axis=1, tiled=True)]
    reduce_sum x1 -> x0, other arithmetic: 3.07 us -> none  [shards(): squares = jnp.sum(piece_wide * piece_wide, axis=1)]
    unnamed x4 -> x5, local copies, waits for them, and re-layouts: 6.83 us -> 8.7 us
  transfers between devices with their start and end apart: 4 -> 0, of which waited for: 4 -> 0; matrix products, arithmetic and copies ran while one was open for 4% -> 0% of each run, Pallas kernels for 0% -> 0%
where the time goes in v1:
time: 170 us; the launch traced here: 169 us
  Pallas kernels  159 us (94%)
  local copies, waits for them, and re-layouts  10.2 us (6%)
    pallas_call x1, Pallas kernels, shards(): pl.pallas_call(functools.partial(kernel, G, n, T, Z, Y, k), out_shape=(ja...  159 us
    unnamed x5, local copies, waits for them, and re-layouts  8.7 us

profile of v1, /device:TPU:0, one launch (start us, length us, event | category | flops | bytes accessed | tf_op | source)
XLA Modules:
  0.0 169.4 jit_solution(15843753631996653627)
XLA Ops:
  0.6 1.5 copy.7.gain_ref
  2.1 158.6 %shard_map.67 = (bf16[256,1024]{1,0:T(8,128)(2,1)}, bf16[2048,1024]{1,0:T(8,128)(2,1)}, bf16[1024,2048]{1,0:T(8,128)(2,1)}) custom-call(bf16[1024,256]{1,0:T(8,128)(2,1)} %tok_ref.1, f32[256,1]{1,0:T(8,128)} %copy.7.gain_ref, f32[256,2048]{1,0:T(8,128)} %upw_ref.1, f32[1024,512]{1,0:T(8,128)} %dnw_ref.1), custom_call_target="tpu_custom_call" | custom-call | tf_op jit(solution)/shard_map/pallas_call | solution.py:364
  160.7 1.9 %copy.11 = bf16[256,1024]{1,0:T(8,128)(2,1)} copy(bf16[256,1024]{1,0:T(8,128)(2,1)} %get-tuple-element.6) | data formatting | bytes 1048576
  162.6 0.0 copy-start
  162.6 4.8 %copy.12 = bf16[2048,1024]{1,0:T(8,128)(2,1)} copy(bf16[2048,1024]{1,0:T(8,128)(2,1)} %get-tuple-element.7) | data formatting | bytes 8388608
  167.4 0.0 copy-done
  167.4 2.0 %copy.13 = bf16[1024,2048]{1,0:T(8,128)(2,1)} copy(bf16[1024,2048]{1,0:T(8,128)(2,1)S(1)} %copy-done) | data formatting | bytes 8388608
Async XLA Ops:
  162.6 4.8 %copy-start = (bf16[1024,2048]{1,0:T(8,128)(2,1)S(1)}, bf16[1024,2048]{1,0:T(8,128)(2,1)}, u32[]{:S(2)}) copy-start(bf16[1024,2048]{1,0:T(8,128)(2,1)} %get-tuple-element.8) | copy-start | bytes 12582916

commit v2 on v1

--- a/solution.py
+++ b/solution.py
@@ -23,12 +23,12 @@
 def kernel(
     G, n, T, Z, Y, k,
     tok_ref, gain_ref, upw_ref, dnw_ref,
-    mixed_ref, up_out, dn_out,
-    up_bf, tok_full, up_full, dn_full, hidden, part, ybuf, zup, zdn,
+    mixed_ref, up_full, dn_full,
+    up_bf, xbuf, tok_full, hidden, part, ybuf, zup, zdn,
     tok_recv, tok_su, tok_sd, tok_sy,
-    up_recv, up_s, up_sx, up_st,
+    x_recv, x_send, up_recv, up_s, up_sx, up_st,
     dn_recv, dn_sx, dn_st,
-    y_recv, y_send, zu_recv, zu_send, zd_recv, zd_send, out_sem,
+    y_recv, y_send, zu_recv, zu_send, zd_recv, zd_send,
 ):
     g, f, t = lax.axis_index("gr"), lax.axis_index("fs"), lax.axis_index("tp")
     z, y = f // Y, f % Y
@@ -82,17 +82,21 @@
     def piece(c, h):
         return up_full.at[pl.ds(pl.multiple_of(c * rows + h * sub, sub), sub)]
 
-    for oh in reversed(range(G)):
+    def to_owner(j, slot, source_q, src):
+        owner = source_q * k + j
+        local = pltpu.make_async_copy(src, piece(f, g), up_recv.at[f, g])
+        pl.when(owner == f)(local.start)
+        send(src, piece(f, g), up_s.at[j, slot], up_recv.at[f, g], (g, owner, t), owner != f)
+
+    def half(j, h):
+        return up_bf.at[j, pl.ds(pl.multiple_of(h * sub, sub), sub)]
+
+    for oh in range(1, G):
         h = (g + oh) % G
         for j in range(k):
-            owner = q * k + j
-            src = up_bf.at[j, pl.ds(pl.multiple_of(h * sub, sub), sub)]
-            if oh == 0:
-                local = pltpu.make_async_copy(src, piece(f, h), up_recv.at[f, h])
-                pl.when(owner == f)(local.start)
-                send(src, piece(f, h), up_s.at[j, oh], up_recv.at[f, h], (h, owner, t), owner != f)
-            else:
-                send(src, piece(f, h), up_s.at[j, oh], up_recv.at[f, h], (h, owner, t))
+            send(half(j, h), xbuf.at[G - oh, j], x_send.at[j, oh], x_recv.at[j, G - oh], (h, f, t))
+    for j in range(k):
+        to_owner(j, 0, q, half(j, g))
 
     def dn_block(index):
         return dn_full.at[:, pl.ds(pl.multiple_of(index * dcols, dcols), dcols)]
@@ -113,27 +117,40 @@
     star = (f // k) % T
     is_star = t == star
 
-    def relay_direct(c):
-        @pl.when(is_star)
+    def relay_direct(c, cond):
+        ok = is_star & cond
+
+        @pl.when(ok)
         def _():
             arrived(piece(c, g), up_recv.at[c, g])
         for o in range(1, G):
-            send(piece(c, g), piece(c, g), up_sx.at[c, o], up_recv.at[c, g], ((g + o) % G, f, t), is_star)
+            send(piece(c, g), piece(c, g), up_sx.at[c, o], up_recv.at[c, g], ((g + o) % G, f, t), ok)
         for o in range(1, T):
-            send(piece(c, g), piece(c, g), up_st.at[c, 0, o], up_recv.at[c, g], (g, f, (t + o) % T), is_star)
-
-    def relay_far(c):
+            send(piece(c, g), piece(c, g), up_st.at[c, 0, o], up_recv.at[c, g], (g, f, (t + o) % T), ok)
+
+    def relay_far(c, cond):
+        ok = is_star & cond
         for oh in range(1, G):
             h = (g + oh) % G
-            @pl.when(is_star)
+
+            @pl.when(ok)
             def _():
                 arrived(piece(c, h), up_recv.at[c, h])
             for o in range(1, T):
-                send(piece(c, h), piece(c, h), up_st.at[c, oh, o], up_recv.at[c, h], (g, f, (t + o) % T), is_star)
+                send(piece(c, h), piece(c, h), up_st.at[c, oh, o], up_recv.at[c, h], (g, f, (t + o) % T), ok)
+
+    for og in range(1, G):
+        for j in range(k):
+            arrived(xbuf.at[og, j], x_recv.at[j, og])
+            to_owner(j, og, ((g + og) % G) * T + t, xbuf.at[og, j])
+    own.wait()
 
     earlier = []
     for s in range(Z):
-        if s > 0:
+        now = []
+        if s == 0:
+            now = [(z * Y + (y + o) % Y, True) for o in range(Y)]
+        else:
             lower, upper = z - s >= 0, z + s < Z
             zl, zu = jnp.maximum(z - s, 0), jnp.minimum(z + s, Z - 1)
 
@@ -148,14 +165,13 @@
                 arrived(tok_full.at[zu * Y + y], tok_recv.at[zu * Y + y])
             pass_tokens(zu, tok_full.at[zu * Y + y], None, upper & (z > 0))
             cross_tokens(zu, tok_full.at[zu * Y + y], upper)
-        else:
-            own.wait()
-        zc = (z + s) % Z
-        now = [zc * Y + (y + o) % Y for o in range(Y)]
-        for c in now:
-            relay_direct(c)
-        for c in earlier:
-            relay_far(c)
+            for o in range(Y):
+                now.append((zl * Y + (y + o) % Y, lower))
+                now.append((zu * Y + (y + o) % Y, upper))
+        for c, cond in now:
+            relay_direct(c, cond)
+        for c, cond in earlier:
+            relay_far(c, cond)
         earlier = now
         if s == 1 % Z:
             for o in range(1, G):
@@ -163,8 +179,8 @@
                 arrived(dn_block(index), dn_recv.at[index])
                 for ot in range(1, T):
                     send(dn_block(index), dn_block(index), dn_st.at[o, ot], dn_recv.at[index], (g, f, (t + ot) % T))
-    for c in earlier:
-        relay_far(c)
+    for c, cond in earlier:
+        relay_far(c, cond)
 
     for zc in range(Z):
         for o in range(1, Y):
@@ -177,9 +193,6 @@
         def _(c):
             for h in range(G):
                 arrived(piece(c, h), up_recv.at[c, h])
-
-    up_store = pltpu.make_async_copy(up_full, up_out, out_sem.at[0])
-    up_store.start()
 
     tokens_here = tok_ref.shape[0]
     tile = chunks(tokens_here, 256)
@@ -202,8 +215,6 @@
         for ot in range(1, T):
             index = ((g + o) % G) * T + (t + ot) % T
             arrived(dn_block(index), dn_recv.at[index])
-    dn_store = pltpu.make_async_copy(dn_full, dn_out, out_sem.at[1])
-    dn_store.start()
 
     feat = part.shape[1]
 
@@ -213,10 +224,6 @@
             order = sorted(range(Z), key=lambda zd: (-abs(zd - zv), zd))
             value = jnp.where(z == zv, order[o], value)
         return value
-
-    def multiply(c):
-        across = dn_full[:, pl.ds(pl.multiple_of(c * feat, feat), feat)] if feat % 128 == 0 else None
-        return across
 
     if feat % 128 == 0:
         def compute(c):
@@ -334,8 +341,6 @@
             copy.wait_send()
         else:
             pl.when(cond)(copy.wait_send)
-    up_store.wait()
-    dn_store.wait()
 
 
 def nth_dynamic(i, z, Z):
@@ -364,28 +369,27 @@
     return pl.pallas_call(
         functools.partial(kernel, G, n, T, Z, Y, k),
         out_shape=(
-            jax.ShapeDtypeStruct((feat, here), bf),
-            jax.ShapeDtypeStruct((width, unit), bf),
-            jax.ShapeDtypeStruct((deep, dcols * G * T), bf),
+            pltpu.VMEM((feat, here), bf),
+            pltpu.VMEM((width, unit), bf),
+            pltpu.VMEM((deep, dcols * G * T), bf),
         ),
         in_specs=[vmem] * 4,
-        out_specs=(vmem, hbm, hbm),
+        out_specs=(vmem, vmem, vmem),
         scratch_shapes=[
             pltpu.VMEM((k, rows, unit), bf),
+            pltpu.VMEM((G, k, rows // G, unit), bf),
             pltpu.VMEM((n, here, w), bf),
-            pltpu.VMEM((width, unit), bf),
-            pltpu.VMEM((deep, dcols * G * T), bf),
             pltpu.VMEM((here, unit), bf),
             pltpu.VMEM((n, feat, here), bf),
             pltpu.VMEM((Z, Y, feat, here), bf),
             pltpu.VMEM((Z, feat, here), bf),
             pltpu.VMEM((Z, feat, here), bf),
             dma((n,)), dma((Z,)), dma((Z,)), dma((Z, Y)),
-            dma((n, G)), dma((k, G)), dma((n, G)), dma((n, G, T)),
+            dma((k, G)), dma((k, G)), dma((n, G)), dma((k, G)), dma((n, G)), dma((n, G, T)),
             dma((G * T,)), dma((G,)), dma((G, T)),
-            dma((Z, Y)), dma((Z, Y)), dma((Z,)), dma((Z,)), dma((Z,)), dma((Z,)), dma((2,)),
+            dma((Z, Y)), dma((Z, Y)), dma((Z,)), dma((Z,)), dma((Z,)), dma((Z,)),
         ],
-        compiler_params=pltpu.CompilerParams(has_side_effects=True, vmem_limit_bytes=60 * 1024 * 1024),
+        compiler_params=pltpu.CompilerParams(has_side_effects=True, vmem_limit_bytes=46 * 1024 * 1024),
     )(tokens, norm_gain[:, None], up_weight, down_weight)
 
 

time: 170 us -> 143 us (0.84)
  Pallas kernels: 159 us -> 135 us
  local copies, waits for them, and re-layouts: 10.2 us -> 6.29 us
    pallas_call x1, Pallas kernels: 159 us -> 135 us  [shards(): pl.pallas_call(functools.partial(kernel, G, n, T, Z, Y, k), out_shape=(pl...]
    unnamed x5 -> x3, local copies, waits for them, and re-layouts: 8.7 us -> 4.82 us
where the time goes in v2:
time: 143 us; the launch traced here: 142 us
  Pallas kernels  135 us (94%)
  local copies, waits for them, and re-layouts  6.29 us (4%)
    pallas_call x1, Pallas kernels, shards(): pl.pallas_call(functools.partial(kernel, G, n, T, Z, Y, k), out_shape=(pl...  135 us
    unnamed x3, local copies, waits for them, and re-layouts  4.82 us

profile of v2, /device:TPU:0, one launch (start us, length us, event | category | flops | bytes accessed | tf_op | source)
XLA Modules:
  0.0 142.4 jit_solution(15411704050971297472)
XLA Ops:
  0.6 1.5 %copy.7.gain_ref = f32[256,1]{1,0:T(8,128)} copy(f32[256,1]{0,1:T(1,128)} %bitcast.1) | data formatting | bytes 2048 | tf_op jit(solution)/shard_map/broadcast_in_dim | solution.py:393
  2.1 135.4 %shard_map.67 = (bf16[256,1024]{1,0:T(8,128)(2,1)S(1)}, bf16[2048,1024]{1,0:T(8,128)(2,1)S(1)}, bf16[1024,2048]{1,0:T(8,128)(2,1)S(1)}) custom-call(bf16[1024,256]{1,0:T(8,128)(2,1)} %tok_ref.1, f32[256,1]{1,0:T(8,128)} %copy.7.gain_ref, f32[256,2048]{1,0:T(8,128)} %upw_ref.1, f32[1024,512]{1,0:T(8,128)} %dnw_ref.1), custom_call_target="tpu_custom_call" | custom-call | tf_op jit(solution)/shard_map/pallas_call | solution.py:369
  137.6 0.8 copy.11
  138.3 2.0 %copy.12 = bf16[2048,1024]{1,0:T(8,128)(2,1)} copy(bf16[2048,1024]{1,0:T(8,128)(2,1)S(1)} %get-tuple-element.4) | data formatting | bytes 8388608
  140.4 2.0 %copy.13 = bf16[1024,2048]{1,0:T(8,128)(2,1)} copy(bf16[1024,2048]{1,0:T(8,128)(2,1)S(1)} %get-tuple-element.5) | data formatting | bytes 8388608

commit v3 on v2

--- a/solution.py
+++ b/solution.py
@@ -21,7 +21,7 @@
 
 
 def kernel(
-    G, n, T, Z, Y, k,
+    G, n, T, Z, Y, k, E,
     tok_ref, gain_ref, upw_ref, dnw_ref,
     mixed_ref, up_full, dn_full,
     up_bf, xbuf, tok_full, hidden, part, ybuf, zup, zdn,
@@ -52,25 +52,35 @@
     def arrived(ref, sem):
         pltpu.make_async_copy(ref, ref, sem).wait()
 
-    own = pltpu.make_async_copy(tok_ref, tok_full.at[f], tok_recv.at[f])
-    own.start()
-
-    def pass_tokens(zc, src, up, down):
+    slab = tok_ref.shape[0] // E
+
+    def owns(e):
+        return pltpu.make_async_copy(tok_ref.at[pl.ds(e * slab, slab)], tok(f, e), tok_recv.at[f, e])
+
+    def tok(c, e):
+        return tok_full.at[c, pl.ds(e * slab, slab)]
+
+    for e in range(E):
+        owns(e).start()
+
+    def pass_tokens(zc, e, src, up, down):
         c = zc * Y + y
-        dst = tok_full.at[c]
+        dst = tok(c, e)
         if up is not None:
-            send(src, dst, tok_su.at[zc], tok_recv.at[c], (g, f + Y, t), up)
+            send(src, dst, tok_su.at[zc, e], tok_recv.at[c, e], (g, f + Y, t), up)
         if down is not None:
-            send(src, dst, tok_sd.at[zc], tok_recv.at[c], (g, f - Y, t), down)
-
-    def cross_tokens(zc, src, cond):
+            send(src, dst, tok_sd.at[zc, e], tok_recv.at[c, e], (g, f - Y, t), down)
+
+    def cross_tokens(zc, e, src, cond):
         c = zc * Y + y
         for o in range(1, Y):
             y2 = (y + o) % Y
-            send(src, tok_full.at[c], tok_sy.at[zc, o], tok_recv.at[c], (g, z * Y + y2, t), cond)
-
-    pass_tokens(z, tok_ref, z < Z - 1, z > 0)
-    cross_tokens(z, tok_ref, None)
+            send(src, tok(c, e), tok_sy.at[zc, o, e], tok_recv.at[c, e], (g, z * Y + y2, t), cond)
+
+    for e in range(E):
+        mine = tok_ref.at[pl.ds(e * slab, slab)]
+        pass_tokens(z, e, mine, z < Z - 1, z > 0)
+        cross_tokens(z, e, mine, None)
 
     step = chunks(rows, 32)
     for j in range(k):
@@ -143,7 +153,8 @@
         for j in range(k):
             arrived(xbuf.at[og, j], x_recv.at[j, og])
             to_owner(j, og, ((g + og) % G) * T + t, xbuf.at[og, j])
-    own.wait()
+    for e in range(E):
+        owns(e).wait()
 
     earlier = []
     for s in range(Z):
@@ -154,17 +165,18 @@
             lower, upper = z - s >= 0, z + s < Z
             zl, zu = jnp.maximum(z - s, 0), jnp.minimum(z + s, Z - 1)
 
-            @pl.when(lower)
-            def _():
-                arrived(tok_full.at[zl * Y + y], tok_recv.at[zl * Y + y])
-            pass_tokens(zl, tok_full.at[zl * Y + y], lower & (z < Z - 1), None)
-            cross_tokens(zl, tok_full.at[zl * Y + y], lower)
-
-            @pl.when(upper)
-            def _():
-                arrived(tok_full.at[zu * Y + y], tok_recv.at[zu * Y + y])
-            pass_tokens(zu, tok_full.at[zu * Y + y], None, upper & (z > 0))
-            cross_tokens(zu, tok_full.at[zu * Y + y], upper)
+            for e in range(E):
+                @pl.when(lower)
+                def _():
+                    arrived(tok(zl * Y + y, e), tok_recv.at[zl * Y + y, e])
+                pass_tokens(zl, e, tok(zl * Y + y, e), lower & (z < Z - 1), None)
+                cross_tokens(zl, e, tok(zl * Y + y, e), lower)
+
+                @pl.when(upper)
+                def _():
+                    arrived(tok(zu * Y + y, e), tok_recv.at[zu * Y + y, e])
+                pass_tokens(zu, e, tok(zu * Y + y, e), None, upper & (z > 0))
+                cross_tokens(zu, e, tok(zu * Y + y, e), upper)
             for o in range(Y):
                 now.append((zl * Y + (y + o) % Y, lower))
                 now.append((zu * Y + (y + o) % Y, upper))
@@ -185,7 +197,8 @@
     for zc in range(Z):
         for o in range(1, Y):
             c = zc * Y + (y + o) % Y
-            arrived(tok_full.at[c], tok_recv.at[c])
+            for e in range(E):
+                arrived(tok(c, e), tok_recv.at[c, e])
 
     @pl.when(jnp.logical_not(is_star))
     def _():
@@ -360,6 +373,7 @@
     deep, dcols = down_weight.shape
     unit = cols * G * T // n
     k = n // (G * T)
+    E = 2 if here % 64 == 0 else 1
     width = rows * n
     feat = dcols * G * T // n
     bf = jnp.bfloat16
@@ -367,7 +381,7 @@
     vmem = pl.BlockSpec(memory_space=pltpu.VMEM)
     hbm = pl.BlockSpec(memory_space=pl.ANY)
     return pl.pallas_call(
-        functools.partial(kernel, G, n, T, Z, Y, k),
+        functools.partial(kernel, G, n, T, Z, Y, k, E),
         out_shape=(
             pltpu.VMEM((feat, here), bf),
             pltpu.VMEM((width, unit), bf),
@@ -384,7 +398,7 @@
             pltpu.VMEM((Z, Y, feat, here), bf),
             pltpu.VMEM((Z, feat, here), bf),
             pltpu.VMEM((Z, feat, here), bf),
-            dma((n,)), dma((Z,)), dma((Z,)), dma((Z, Y)),
+            dma((n, E)), dma((Z, E)), dma((Z, E)), dma((Z, Y, E)),
             dma((k, G)), dma((k, G)), dma((n, G)), dma((k, G)), dma((n, G)), dma((n, G, T)),
             dma((G * T,)), dma((G,)), dma((G, T)),
             dma((Z, Y)), dma((Z, Y)), dma((Z,)), dma((Z,)), dma((Z,)), dma((Z,)),

time: 143 us -> 141 us (0.986)
    pallas_call x1, Pallas kernels: 135 us -> 134 us  [shards(): pl.pallas_call(functools.partial(kernel, G, n, T, Z, Y, k, E), out_shape=...]
where the time goes in v3:
time: 141 us
  Pallas kernels  134 us (95%)
  local copies, waits for them, and re-layouts  6.29 us (4%)
    pallas_call x1, Pallas kernels, shards(): pl.pallas_call(functools.partial(kernel, G, n, T, Z, Y, k, E), out_shape=...  134 us
    unnamed x3, local copies, waits for them, and re-layouts  4.82 us

profile of v3, /device:TPU:0, one launch (start us, length us, event | category | flops | bytes accessed | tf_op | source)
XLA Modules:
  0.0 140.6 jit_solution(10537890352739598059)
XLA Ops:
  0.6 1.5 %copy.7.gain_ref = f32[256,1]{1,0:T(8,128)} copy(f32[256,1]{0,1:T(1,128)} %bitcast.1) | data formatting | bytes 2048 | tf_op jit(solution)/shard_map/broadcast_in_dim | solution.py:407
  2.1 133.7 %shard_map.67 = (bf16[256,1024]{1,0:T(8,128)(2,1)S(1)}, bf16[2048,1024]{1,0:T(8,128)(2,1)S(1)}, bf16[1024,2048]{1,0:T(8,128)(2,1)S(1)}) custom-call(bf16[1024,256]{1,0:T(8,128)(2,1)} %tok_ref.1, f32[256,1]{1,0:T(8,128)} %copy.7.gain_ref, f32[256,2048]{1,0:T(8,128)} %upw_ref.1, f32[1024,512]{1,0:T(8,128)} %dnw_ref.1), custom_call_target="tpu_custom_call" | custom-call | tf_op jit(solution)/shard_map/pallas_call | solution.py:383
  135.8 0.8 copy.11
  136.6 2.0 %copy.12 = bf16[2048,1024]{1,0:T(8,128)(2,1)} copy(bf16[2048,1024]{1,0:T(8,128)(2,1)S(1)} %get-tuple-element.4) | data formatting | bytes 8388608
  138.6 2.0 %copy.13 = bf16[1024,2048]{1,0:T(8,128)(2,1)} copy(bf16[1024,2048]{1,0:T(8,128)(2,1)S(1)} %get-tuple-element.5) | data formatting | bytes 8388608
